TPU v7x, 32 devices: a whole 2x2x4 slice. The times are simulated.
32 devices in a mesh: sp: 8 (over z, y), tp: 4 (over x, core).
Axes of the slice: x: 2, y: 2, z: 4, core: 2. Of those that a mesh axis runs over, the one named last changes fastest.
Arguments:
- resid: bfloat16 [2048, 2048], P(('sp', 'tp')), may hold values from -6 to 6
- query_a: bfloat16 [2048, 4, 128], P('sp', 'tp')
- key_a: bfloat16 [2048, 4, 128], P('sp', 'tp')
- value_a: bfloat16 [2048, 4, 128], P('sp', 'tp'), may hold values from -6 to 6
- query_b: bfloat16 [2048, 4, 256], P('sp', 'tp')
- key_b: bfloat16 [2048, 4, 256], P('sp', 'tp')
- value_b: bfloat16 [2048, 4, 128], P('sp', 'tp'), may hold values from -6 to 6
- lambda_a: float32 [4], P('tp'), may hold values from 0.3 to 0.8
- lambda_b: float32 [4], P('tp'), may hold values from 0.3 to 0.8
- head_gain: float32 [128], replicated, may hold values from 0.1 to 1.9
- out_weight: bfloat16 [1024, 2048], replicated, may hold values from -0.1875 to 0.1875
- norm_gain: float32 [2048], replicated, may hold values from 0.1 to 1.9
- expert_ids: int32 [2048, 4], P(('sp', 'tp')), may hold values from 0 to 31, all different within a row; in each aligned block of 64 rows (0 to 63, 64 to 127, ...) at most 16 rows name the same one
- expert_mix: float32 [2048, 4], P(('sp', 'tp')), may hold values from 0.2 to 1
- gate_experts: bfloat16 [32, 2048, 1024], P(('sp', 'tp')), may hold values from -0.125 to 0.125
- up_experts: bfloat16 [32, 2048, 1024], P(('sp', 'tp')), may hold values from -0.125 to 0.125
- down_experts: bfloat16 [32, 1024, 2048], P(('sp', 'tp')), may hold values from -0.1875 to 0.1875
- shared_gate: bfloat16 [2048, 512], replicated, may hold values from -0.125 to 0.125
- shared_up: bfloat16 [2048, 512], replicated, may hold values from -0.125 to 0.125
- shared_down: bfloat16 [512, 2048], replicated, may hold values from -0.25 to 0.25
Outputs:
- layer_out: bfloat16 [2048, 2048], P(('sp', 'tp'))
Inputs may be any that keep to these rules, and one draw needn't show every extreme that they name: `expert_ids`: in each aligned block of 64 rows (the rows of one device) no expert is named more than 16 times, a bound that some block reaches.
All inputs are finite; a program needn't handle non-finite values.
Results may differ from a plain program's by a relative error of at most 0.017.
Values may be sent and summed in bfloat16 or wider, within the bound.
No kernel may reach another device: no remote copies, remote signals or barrier semaphores. Data moves between devices by JAX's collectives and lax.ppermute only.
A program may use at most 128 MiB of HBM per device.

v0:
```python
import math
import jax
import jax.numpy as jnp
from jax import lax
from jax.sharding import PartitionSpec as P

NEG_FILL = -1e30
EPSILON = 1e-05
HEAD_SCALE = 0.8
KEY_SPAN = 2048


def swiglu_rows(row_set, w_gate, w_up, w_down):
    gate_val = jnp.dot(row_set, w_gate, preferred_element_type=jnp.float32)
    up_val = jnp.dot(row_set, w_up, preferred_element_type=jnp.float32)
    hidden = (jax.nn.silu(gate_val) * up_val).astype(jnp.bfloat16)
    return jnp.dot(hidden, w_down, preferred_element_type=jnp.float32)


def online_update(state, query_map, key_map, value_block, causal, scaling):
    row_top, denoms, numerator = state
    scores = (
        jnp.einsum("qhd,khd->hqk", query_map, key_map, preferred_element_type=jnp.float32) * scaling
    )
    scores = jnp.where(causal, scores, NEG_FILL)
    new_top = jnp.maximum(row_top, jnp.max(scores, axis=2))
    exponent = jnp.where(causal, jnp.exp(scores - new_top[:, :, None]), 0.0)
    shrink = jnp.exp(row_top - new_top)
    denoms = denoms * shrink + jnp.sum(exponent, axis=2)
    numerator = numerator * jnp.transpose(shrink)[:, :, None] + jnp.einsum(
        "hqk,khe->qhe",
        exponent.astype(jnp.bfloat16),
        value_block,
        preferred_element_type=jnp.float32,
    )
    return (new_top, denoms, numerator)


def group_update(states, queries, key_block, value_block, causal):
    map_width = queries.shape[2] // 2
    scaling = map_width ** (-0.5)
    first_state = online_update(
        states[0],
        queries[:, :, :map_width],
        key_block[:, :, :map_width],
        value_block,
        causal,
        scaling,
    )
    second_state = online_update(
        states[1],
        queries[:, :, map_width:],
        key_block[:, :, map_width:],
        value_block,
        causal,
        scaling,
    )
    return (first_state, second_state)


def empty_state(query_rows, head_count, value_width):
    single = (
        jnp.full((head_count, query_rows), NEG_FILL, jnp.float32),
        jnp.zeros((head_count, query_rows), jnp.float32),
        jnp.zeros((query_rows, head_count, value_width), jnp.float32),
    )
    return (single, single)


def finish_group(states, lambdas, head_gain):
    first_out = states[0][2] / jnp.transpose(states[0][1])[:, :, None]
    second_out = states[1][2] / jnp.transpose(states[1][1])[:, :, None]
    differ = first_out - lambdas[None, :, None] * second_out
    scale_rms = lax.rsqrt(jnp.mean(differ * differ, axis=2, keepdims=True) + EPSILON)
    return (differ * scale_rms * head_gain[None, None, :] * HEAD_SCALE).astype(jnp.bfloat16)


def per_device(
    resid,
    query_a,
    key_a,
    value_a,
    query_b,
    key_b,
    value_b,
    lambda_a,
    lambda_b,
    head_gain,
    out_weight,
    norm_gain,
    expert_ids,
    expert_mix,
    gate_experts,
    up_experts,
    down_experts,
    shared_gate,
    shared_up,
    shared_down,
):
    query_rows = query_a.shape[0]
    value_width = value_a.shape[2]
    query_pos = lax.axis_index("sp") * query_rows + jnp.arange(query_rows, dtype=jnp.int32)
    start_state = (
        empty_state(query_rows, query_a.shape[1], value_width),
        empty_state(query_rows, query_b.shape[1], value_width),
    )
    key_piece_a = lax.all_gather(key_a, "sp", axis=0, tiled=True)
    value_piece_a = lax.all_gather(value_a, "sp", axis=0, tiled=True)
    key_piece_b = lax.all_gather(key_b, "sp", axis=0, tiled=True)
    value_piece_b = lax.all_gather(value_b, "sp", axis=0, tiled=True)
    piece_rows = key_piece_a.shape[0]
    step_rows = math.gcd(piece_rows, KEY_SPAN)

    def one_step(step_index, inner_state):
        begin_row = step_index * step_rows
        key_pos = begin_row + jnp.arange(step_rows, dtype=jnp.int32)
        causal = (key_pos[None, :] <= query_pos[:, None])[None]
        part_a = group_update(
            inner_state[0],
            query_a,
            lax.dynamic_slice_in_dim(key_piece_a, begin_row, step_rows, 0),
            lax.dynamic_slice_in_dim(value_piece_a, begin_row, step_rows, 0),
            causal,
        )
        part_b = group_update(
            inner_state[1],
            query_b,
            lax.dynamic_slice_in_dim(key_piece_b, begin_row, step_rows, 0),
            lax.dynamic_slice_in_dim(value_piece_b, begin_row, step_rows, 0),
            causal,
        )
        return (part_a, part_b)

    state_a, state_b = lax.fori_loop(0, piece_rows // step_rows, one_step, start_state)
    heads_a = finish_group(state_a, lambda_a, head_gain)
    heads_b = finish_group(state_b, lambda_b, head_gain)
    tok_dev = resid.shape[0]
    back_a, back_b = (
        lax.all_to_all(heads_a, "tp", split_axis=0, concat_axis=1, tiled=True),
        lax.all_to_all(heads_b, "tp", split_axis=0, concat_axis=1, tiled=True),
    )
    joined = jnp.concatenate([back_a.reshape(tok_dev, -1), back_b.reshape(tok_dev, -1)], axis=1)
    project = jnp.dot(joined, out_weight, preferred_element_type=jnp.float32)
    middle = (resid.astype(jnp.float32) + project).astype(jnp.bfloat16)
    middle_f = middle.astype(jnp.float32)
    normed = (
        middle_f
        * lax.rsqrt(jnp.mean(middle_f * middle_f, axis=1, keepdims=True) + EPSILON)
        * norm_gain[None, :]
    ).astype(jnp.bfloat16)
    shared = swiglu_rows(normed, shared_gate, shared_up, shared_down)
    top_count = expert_ids.shape[1]
    model_width = normed.shape[1]
    sp_count = lax.axis_size("sp")
    tp_count = lax.axis_size("tp")
    expert_total = sp_count * tp_count
    pair_count = tok_dev * top_count
    capacity = max(2, 2 * pair_count // expert_total)
    flat_ids = expert_ids.reshape(-1)
    one_hot = (flat_ids[:, None] == jnp.arange(expert_total, dtype=jnp.int32)[None, :]).astype(
        jnp.int32
    )
    pair_rank = jnp.sum((jnp.cumsum(one_hot, axis=0) - one_hot) * one_hot, axis=1)
    pair_token = jnp.arange(pair_count, dtype=jnp.int32) // top_count
    send_rows = (
        jnp.zeros((expert_total, capacity, model_width), jnp.bfloat16)
        .at[flat_ids, pair_rank]
        .set(normed[pair_token])
    )
    arrived = lax.all_to_all(send_rows, ("sp", "tp"), split_axis=0, concat_axis=0, tiled=True)
    arrived_shape = arrived.shape
    flat_rows = arrived.reshape(-1, arrived_shape[-1])
    result = swiglu_rows(flat_rows, gate_experts[0], up_experts[0], down_experts[0]).astype(
        jnp.bfloat16
    )
    finished = result.reshape(arrived_shape)
    returned = lax.all_to_all(finished, ("sp", "tp"), split_axis=0, concat_axis=0, tiled=True)
    chosen = returned[flat_ids, pair_rank].reshape(tok_dev, top_count, model_width)
    routed = jnp.sum(chosen.astype(jnp.float32) * expert_mix[:, :, None], axis=1)
    return (middle_f + shared + routed).astype(jnp.bfloat16)


def solution(mesh):
    in_specs = (
        P(("sp", "tp"), None),
        P("sp", "tp", None),
        P("sp", "tp", None),
        P("sp", "tp", None),
        P("sp", "tp", None),
        P("sp", "tp", None),
        P("sp", "tp", None),
        P("tp"),
        P("tp"),
        P(),
        P(),
        P(),
        P(("sp", "tp"), None),
        P(("sp", "tp"), None),
        P(("sp", "tp"), None, None),
        P(("sp", "tp"), None, None),
        P(("sp", "tp"), None, None),
        P(),
        P(),
        P(),
    )
    out_specs = P(("sp", "tp"), None)
    return jax.shard_map(
        per_device, mesh=mesh, in_specs=in_specs, out_specs=out_specs, check_vma=False
    )
```

profile of v0, /device:TPU:0, one launch (start us, length us, event | category | flops | bytes accessed | tf_op | source)
XLA Modules:
  0.0 333.9 jit_solution(18437636033774966400)
XLA Ops:
  6.5 0.7 all-gather.2.cloned.1.call-update
  7.3 33.6 %all_gather.12 = bf16[2048,1,128]{2,0,1:T(8,128)(2,1)S(1)} all-gather(bf16[256,1,128]{2,0,1:T(8,128)(2,1)} %param.22), channel_id=1, replica_groups=mesh['sp'=8,'tp'=4] {'sp'}, dimensions={0}, use_global_device_ids=true | all-gather | bytes 589824 | tf_op jit(solution)/shard_map/all_gather | solution.py:107
  40.9 0.8 copy.35
  41.6 0.1 eq.29
  41.8 0.6 reduce-window.6
  42.4 0.2 slice_reduce_fusion
  42.6 0.1 eq.25
  42.7 0.1 reshape.406
  44.1 0.1 fusion.73
  44.2 2.8 fusion.88
  47.0 1.8 fusion.89
  48.9 31.4 %all_gather.15 = bf16[2048,1,128]{2,0,1:T(8,128)(2,1)S(1)} all-gather(bf16[256,1,128]{2,0,1:T(8,128)(2,1)S(1)} %copy-done.5), channel_id=1, replica_groups=mesh['sp'=8,'tp'=4] {'sp'}, dimensions={0}, use_global_device_ids=true | all-gather | bytes 589824 | tf_op jit(solution)/shard_map/all_gather | solution.py:110
  80.3 31.5 %all_gather.13 = bf16[2048,1,128]{2,0,1:T(8,128)(2,1)S(1)} all-gather(bf16[256,1,128]{2,0,1:T(8,128)(2,1)S(1)} %copy-done.6), channel_id=1, replica_groups=mesh['sp'=8,'tp'=4] {'sp'}, dimensions={0}, use_global_device_ids=true | all-gather | bytes 589824 | tf_op jit(solution)/shard_map/all_gather | solution.py:108
  111.8 1.8 fusion.91
  113.6 1.8 fusion.90
  115.4 2.1 fusion.19
  117.5 0.7 fusion.38
  118.2 0.7 multiply_reduce_fusion.2
  118.9 0.7 fusion.32
  119.6 0.7 multiply_reduce_fusion.3
  120.4 0.6 broadcast.531
  121.0 0.7 reduce.22
  121.7 0.1 copy.50
  121.8 0.7 reshape.432
  122.5 3.3 all-to-all-start.1
  125.8 0.7 reduce.23
  126.5 0.1 copy.51
  126.6 0.6 reshape.434
  127.3 2.6 all-to-all-done.1
  129.9 3.3 all-to-all-start
  133.3 3.9 %all-to-all-done = bf16[4,2,4096]{2,1,0:T(2,128)(2,1)S(1)} async-done(((bf16[4,2,4096]{2,1,0:T(2,128)(2,1)}), bf16[4,2,4096]{2,1,0:T(2,128)(2,1)S(1)}, u32[]{:S(2)}, u32[]{:S(2)}) %all-to-all-start) | async-done | bytes 65568 | tf_op jit(solution)/shard_map/all_to_all | solution.py:139
  137.4 3.2 multiply_reduce_fusion.1
  140.6 0.1 multiply_convert_fusion.1
  140.7 2.3 gather_fusion
  143.1 1.6 broadcast_in_dim.49
  144.7 46.2 %scatter_fusion = bf16[32,16,2048]{2,1,0:T(8,128)(2,1)} fusion(bf16[32,16,2048]{2,1,0:T(8,128)(2,1)} %broadcast_in_dim.49, s32[256]{0:T(256)S(1)} %bitcast.169, bf16[256,2048]{1,0:T(8,128)(2,1)} %gather_fusion), kind=kCustom, calls=%fused_computation.2 | custom fusion | bytes 3147776 | tf_op jit(solution)/shard_map/scatter | solution.py:168
  190.9 53.7 %all_to_all.40 = bf16[32,16,2048]{2,1,0:T(8,128)(2,1)S(1)} all-to-all(bf16[32,16,2048]{2,1,0:T(8,128)(2,1)} %scatter_fusion), channel_id=1, replica_groups=mesh['sp'=8,'tp'=4] {'sp','tp'}, dimensions={0} | all-to-all | bytes 4194304 | tf_op jit(solution)/shard_map/all_to_all | solution.py:170
  244.6 1.3 copy-done.3
  246.0 3.6 %fusion.4 = f32[512,1024]{1,0:T(8,128)} fusion(bf16[512,2048]{1,0:T(8,128)(2,1)S(1)} %bitcast.171, bf16[1,2048,1024]{2,1,0:T(8,128)(2,1)S(1)} %copy-done.10), kind=kOutput, calls=%fused_computation.7 | convolution fusion | flops 2147483648 | bytes 8388608 | tf_op jit(solution)/shard_map/dot_general | solution.py:14
  249.6 10.6 %fusion.6 = bf16[512,2048]{1,0:T(8,128)(2,1)} fusion(bf16[1,1024,2048]{2,1,0:T(8,128)(2,1)} %param.36, f32[512,1024]{1,0:T(8,128)} %fusion.4, bf16[512,2048]{1,0:T(8,128)(2,1)} %bitcast.172, bf16[1,2048,1024]{2,1,0:T(8,128)(2,1)} %param.35), kind=kOutput, calls=%fused_computation.9 | convolution fusion | flops 4299161600 | bytes 14680064 | tf_op jit(solution)/shard_map/dot_general | solution.py:17
  260.2 3.8 %all-to-all-start.3 = ((bf16[32,16,2048]{2,1,0:T(8,128)(2,1)}), bf16[32,16,2048]{2,1,0:T(8,128)(2,1)}, u32[]{:S(2)}, u32[]{:S(2)}) async-start(bf16[32,16,2048]{2,1,0:T(8,128)(2,1)} %bitcast.170), calls=%async_computation.3 | async-start | bytes 4194304 | tf_op jit(solution)/shard_map/all_to_all | solution.py:177
  264.0 0.7 copy.39
  264.7 2.1 fusion.92
  266.8 45.9 %all-to-all-done.3 = bf16[32,16,2048]{2,1,0:T(8,128)(2,1)} async-done(((bf16[32,16,2048]{2,1,0:T(8,128)(2,1)}), bf16[32,16,2048]{2,1,0:T(8,128)(2,1)}, u32[]{:S(2)}, u32[]{:S(2)}) %all-to-all-start.3) | async-done | bytes 2097184 | tf_op jit(solution)/shard_map/all_to_all | solution.py:177
  312.7 5.1 %gather_fusion.1 = bf16[256,2048]{1,0:T(8,128)(2,1)} fusion(bf16[32,16,2048]{2,1,0:T(8,128)(2,1)} %all-to-all-done.3, s32[256]{0:T(256)S(1)} %bitcast.168), kind=kCustom, calls=%fused_computation.1 | custom fusion | bytes 2099200 | tf_op jit(solution)/shard_map/gather | solution.py:178
  317.9 2.7 reshape.410
  320.6 3.2 multiply_reduce_fusion
  323.8 3.2 fusion.14
  (52 shorter events, 0.6 us)
Async XLA Ops:
  6.5 317.3 %copy-start = (bf16[512,2048]{1,0:T(8,128)(2,1)S(1)}, bf16[512,2048]{1,0:T(8,128)(2,1)}, u32[]{:S(2)}) copy-start(bf16[512,2048]{1,0:T(8,128)(2,1)} %param.39) | copy-start | bytes 6291460
  6.5 40.5 %copy-start.12 = (bf16[256,1,128]{2,0,1:T(8,128)(2,1)S(1)}, bf16[256,1,128]{2,0,1:T(8,128)(2,1)}, u32[]{:S(2)}) copy-start(bf16[256,1,128]{2,0,1:T(8,128)(2,1)} %param.21) | copy-start | bytes 196612
  6.5 105.2 %all-gather.2.cloned.1.call-start = ((), (), s32[]{:S(2)}) async-start(), calls=%async_computation.4 | async-start | bytes 1179648 | tf_op jit(solution)/shard_map/all_gather | solution.py:109
  47.0 1.9 copy-start.5
  47.0 33.3 %copy-start.6 = (bf16[256,1,128]{2,0,1:T(8,128)(2,1)S(1)}, bf16[256,1,128]{2,0,1:T(8,128)(2,1)}, u32[]{:S(2)}) copy-start(bf16[256,1,128]{2,0,1:T(8,128)(2,1)} %param.23) | copy-start | bytes 196612
  47.0 64.8 %copy-start.11 = (bf16[256,1,256]{2,0,1:T(8,128)(2,1)S(1)}, bf16[256,1,256]{2,0,1:T(8,128)(2,1)}, u32[]{:S(2)}) copy-start(bf16[256,1,256]{2,0,1:T(8,128)(2,1)} %param.24) | copy-start | bytes 393220
  111.8 3.6 %copy-start.2 = (f32[256,2048]{1,0:T(8,128)S(1)}, f32[256,2048]{1,0:T(8,128)}, u32[]{:S(2)}) copy-start(f32[256,2048]{1,0:T(8,128)} %get-tuple-element.62) | copy-start | bytes 6291460
  113.6 1.8 copy-start.1
  119.6 0.7 copy-start.9
  120.3 17.1 %copy-start.4 = (bf16[64,2048]{1,0:T(8,128)(2,1)S(1)}, bf16[64,2048]{1,0:T(8,128)(2,1)}, u32[]{:S(2)}) copy-start(bf16[64,2048]{1,0:T(8,128)(2,1)} %param.20) | copy-start | bytes 786436
  122.5 7.4 %all-to-all-start.1 = ((bf16[4,2,4096]{2,1,0:T(2,128)(2,1)}), bf16[4,2,4096]{2,1,0:T(2,128)(2,1)S(1)}, u32[]{:S(2)}, u32[]{:S(2)}) async-start(bf16[4,2,4096]{2,1,0:T(2,128)(2,1)} %reshape.432), calls=%async_computation.1 | async-start | bytes 131072 | tf_op jit(solution)/shard_map/all_to_all | solution.py:140
  129.9 7.4 %all-to-all-start = ((bf16[4,2,4096]{2,1,0:T(2,128)(2,1)}), bf16[4,2,4096]{2,1,0:T(2,128)(2,1)S(1)}, u32[]{:S(2)}, u32[]{:S(2)}) async-start(bf16[4,2,4096]{2,1,0:T(2,128)(2,1)} %reshape.434), calls=%async_computation | async-start | bytes 131072 | tf_op jit(solution)/shard_map/all_to_all | solution.py:139
  137.4 3.2 copy-start.7
  190.9 55.0 %copy-start.10 = (bf16[1,2048,1024]{2,1,0:T(8,128)(2,1)S(1)}, bf16[1,2048,1024]{2,1,0:T(8,128)(2,1)}, u32[]{:S(2)}) copy-start(bf16[1,2048,1024]{2,1,0:T(8,128)(2,1)} %param.34) | copy-start | bytes 12582916
  244.6 1.3 copy-start.3
  260.2 3.8 %copy-start.8 = (f32[64,4]{0,1:T(4,128)S(1)}, f32[64,4]{0,1:T(4,128)}, u32[]{:S(2)}) copy-start(f32[64,4]{0,1:T(4,128)} %param.33) | copy-start | bytes 3076
  260.2 52.5 %all-to-all-start.3 = ((bf16[32,16,2048]{2,1,0:T(8,128)(2,1)}), bf16[32,16,2048]{2,1,0:T(8,128)(2,1)}, u32[]{:S(2)}, u32[]{:S(2)}) async-start(bf16[32,16,2048]{2,1,0:T(8,128)(2,1)} %bitcast.170), calls=%async_computation.3 | async-start | bytes 4194304 | tf_op jit(solution)/shard_map/all_to_all | solution.py:177
Sparse Core Ops, SparseCore 0:
  9.5 43.6 all-gather.1
where the time goes:
time: 336 us; the launch traced here: 334 us
  blocking collectives  150 us (45%)
  local copies, waits for them, and re-layouts  63.9 us (19%)
  waiting for transfers between devices  53.1 us (16%)
  matrix products  33.6 us (10%)
  between operations  15.1 us (4%)
  starting transfers between devices  10.4 us (3%)
  other arithmetic  7.7 us (2%)
    all_to_all x1, blocking collectives, per_device(): lax.all_to_all(send_rows, ('sp', 'tp'), split_axis=0, concat_axis=0, tile...  53.7 us
    scatter x1, local copies, waits for them, and re-layouts, per_device(): send_rows = jnp.zeros((expert_total, capacity, model_width), jnp.bfloat16...  46.2 us
    all_to_all x1, waiting for transfers between devices, per_device(): lax.all_to_all(finished, ('sp', 'tp'), split_axis=0, concat_axis=0, tiled...  45.9 us
    all_gather x1, blocking collectives, per_device(): key_piece_a = lax.all_gather(key_a, 'sp', axis=0, tiled=True)  33.6 us
    all_gather x1, blocking collectives, per_device(): value_piece_a = lax.all_gather(value_a, 'sp', axis=0, tiled=True)  31.5 us
    all_gather x1, blocking collectives, per_device(): value_piece_b = lax.all_gather(value_b, 'sp', axis=0, tiled=True)  31.4 us
    dot_general x2, matrix products, swiglu_rows(): return jnp.dot(hidden, w_down, preferred_element_type=jnp.float32)  13.8 us
    dot_general x4, matrix products, online_update(): jnp.einsum('qhd,khd->hqk', query_map, key_map, preferred_element_type=jnp...  8.17 us
  transfers between devices with their start and end apart: 4, of which 3 were waited for; matrix products, arithmetic and copies ran while one was open for 3% of the time, Pallas kernels for 0%

commit v1 on v0

--- a/solution.py
+++ b/solution.py
@@ -97,6 +97,11 @@
     shared_up,
     shared_down,
 ):
+
+    def scan_table_now(q_in, tile_in, bus_axis):
+        item_now = lax.all_gather(jnp.concatenate([q_in, tile_in], 1), bus_axis, axis=0, tiled=True)
+        return jnp.split(item_now, [q_in.shape[1]], 1)
+
     query_rows = query_a.shape[0]
     value_width = value_a.shape[2]
     query_pos = lax.axis_index("sp") * query_rows + jnp.arange(query_rows, dtype=jnp.int32)
@@ -104,8 +109,7 @@
         empty_state(query_rows, query_a.shape[1], value_width),
         empty_state(query_rows, query_b.shape[1], value_width),
     )
-    key_piece_a = lax.all_gather(key_a, "sp", axis=0, tiled=True)
-    value_piece_a = lax.all_gather(value_a, "sp", axis=0, tiled=True)
+    key_piece_a, value_piece_a = scan_table_now(key_a, value_a, "sp")
     key_piece_b = lax.all_gather(key_b, "sp", axis=0, tiled=True)
     value_piece_b = lax.all_gather(value_b, "sp", axis=0, tiled=True)
     piece_rows = key_piece_a.shape[0]

time: 336 us -> 317 us (0.943)
  blocking collectives: 150 us -> 86.2 us
  waiting for transfers between devices: 53.1 us -> 97.3 us
    all_gather x2 -> x0, blocking collectives: 65.1 us -> none  [the longest x1 33.6 us: per_device(): key_piece_a = lax.all_gather(key_a, 'sp', axis=0, tiled=True)]
    all_gather x1, waiting for transfers between devices: 0.01 us -> 36.3 us  [per_device(): key_piece_b = lax.all_gather(key_b, 'sp', axis=0, tiled=True)]
    all_gather x0 -> x1, waiting for transfers between devices: none -> 7.84 us  [scan_table_now(): lax.all_gather(jnp.concatenate([q_in, tile_in], 1), bus_axis, axis=0, til...]
  transfers between devices with their start and end apart: 4 -> 5, of which waited for: 3 -> 5; matrix products, arithmetic and copies ran while one was open for 3% -> 4% of each run, Pallas kernels for 0% -> 0%
where the time goes in v1:
time: 317 us; the launch traced here: 316 us
  waiting for transfers between devices  97.3 us (31%)
  blocking collectives  86.2 us (27%)
  local copies, waits for them, and re-layouts  64.5 us (20%)
  matrix products  33.2 us (10%)
  between operations  15.1 us (5%)
  starting transfers between devices  10.3 us (3%)
  other arithmetic  8.82 us (3%)
    all_to_all x1, blocking collectives, per_device(): lax.all_to_all(send_rows, ('sp', 'tp'), split_axis=0, concat_axis=0, tile...  51.9 us
    scatter x1, local copies, waits for them, and re-layouts, per_device(): send_rows = jnp.zeros((expert_total, capacity, model_width), jnp.bfloat16...  46.2 us
    all_to_all x1, waiting for transfers between devices, per_device(): lax.all_to_all(finished, ('sp', 'tp'), split_axis=0, concat_axis=0, tiled...  45.9 us
    all_gather x1, waiting for transfers between devices, per_device(): key_piece_b = lax.all_gather(key_b, 'sp', axis=0, tiled=True)  36.3 us
    all_gather x1, blocking collectives, per_device(): value_piece_b = lax.all_gather(value_b, 'sp', axis=0, tiled=True)  34.4 us
    dot_general x2, matrix products, swiglu_rows(): return jnp.dot(hidden, w_down, preferred_element_type=jnp.float32)  13.8 us
    dot_general x4, matrix products, online_update(): jnp.einsum('qhd,khd->hqk', query_map, key_map, preferred_element_type=jnp...  8.31 us
    all_gather x1, waiting for transfers between devices, scan_table_now(): lax.all_gather(jnp.concatenate([q_in, tile_in], 1), bus_axis, axis=0, til...  7.84 us
  transfers between devices with their start and end apart: 5, of which 5 were waited for; matrix products, arithmetic and copies ran while one was open for 4% of the time, Pallas kernels for 0%

profile of v1, /device:TPU:0, one launch (start us, length us, event | category | flops | bytes accessed | tf_op | source)
XLA Modules:
  0.0 315.5 jit_solution(1134472638227759348)
XLA Ops:
  6.5 1.7 pad_maximum_fusion
  8.3 0.7 all-gather.5.cloned.1.call-update
  9.0 0.8 copy.41
  9.8 0.1 eq.29
  10.0 0.1 reshape.406
  11.4 0.6 reduce-window.6
  12.0 0.2 slice_reduce_fusion
  12.4 34.4 %all_gather.11 = bf16[2048,1,128]{2,0,1:T(8,128)(2,1)S(1)} all-gather(bf16[256,1,128]{2,0,1:T(8,128)(2,1)} %param.26), channel_id=1, replica_groups=mesh['sp'=8,'tp'=4] {'sp'}, dimensions={0}, use_global_device_ids=true | all-gather | bytes 589824 | tf_op jit(solution)/shard_map/all_gather | solution.py:114
  46.7 7.8 %all-gather.3.cloned.1.call-done = bf16[2048,2,128]{2,0,1:T(8,128)(2,1)} async-done(((bf16[256,2,128]{2,0,1:T(8,128)(2,1)}), bf16[2048,2,128]{2,0,1:T(8,128)(2,1)}) %all-gather.3.cloned.1.call-update) | async-done | bytes 1048592 | tf_op jit(solution)/shard_map/all_gather | solution.py:102
  54.6 3.1 fusion.94
  57.7 1.8 fusion.95
  59.5 36.3 %all-gather.5.cloned.1.call-done = bf16[2048,1,256]{2,0,1:T(8,128)(2,1)} async-done(((bf16[256,1,256]{2,0,1:T(8,128)(2,1)}), bf16[2048,1,256]{2,0,1:T(8,128)(2,1)}) %all-gather.5.cloned.1.call-update) | async-done | bytes 1048592 | tf_op jit(solution)/shard_map/all_gather | solution.py:113
  95.8 1.7 fusion.97
  97.5 1.7 fusion.96
  99.3 1.5 fusion.21
  100.8 0.6 fusion.40
  101.4 0.6 multiply_reduce_fusion.2
  102.1 0.6 copy-done.10
  102.6 0.5 fusion.34
  103.2 0.5 multiply_reduce_fusion.3
  103.9 0.6 broadcast.534
  104.5 0.7 reduce.22
  105.2 0.1 copy.58
  105.3 0.7 reshape.432
  106.0 3.3 %all-to-all-start.1 = ((bf16[4,2,4096]{2,1,0:T(2,128)(2,1)}), bf16[4,2,4096]{2,1,0:T(2,128)(2,1)S(1)}, u32[]{:S(2)}, u32[]{:S(2)}) async-start(bf16[4,2,4096]{2,1,0:T(2,128)(2,1)} %reshape.432), calls=%async_computation.1 | async-start | bytes 131072 | tf_op jit(solution)/shard_map/all_to_all | solution.py:144
  109.3 0.7 reduce.23
  110.0 0.1 copy.59
  110.1 0.6 reshape.434
  110.8 2.6 all-to-all-done.1
  113.4 3.3 %all-to-all-start = ((bf16[4,2,4096]{2,1,0:T(2,128)(2,1)}), bf16[4,2,4096]{2,1,0:T(2,128)(2,1)S(1)}, u32[]{:S(2)}, u32[]{:S(2)}) async-start(bf16[4,2,4096]{2,1,0:T(2,128)(2,1)} %reshape.434), calls=%async_computation | async-start | bytes 131072 | tf_op jit(solution)/shard_map/all_to_all | solution.py:143
  116.8 3.9 %all-to-all-done = bf16[4,2,4096]{2,1,0:T(2,128)(2,1)S(1)} async-done(((bf16[4,2,4096]{2,1,0:T(2,128)(2,1)}), bf16[4,2,4096]{2,1,0:T(2,128)(2,1)S(1)}, u32[]{:S(2)}, u32[]{:S(2)}) %all-to-all-start) | async-done | bytes 65568 | tf_op jit(solution)/shard_map/all_to_all | solution.py:143
  120.9 3.2 %multiply_reduce_fusion.1 = (f32[64]{0:T(128)S(1)}, f32[64,2048]{1,0:T(8,128)S(1)}) fusion(bf16[1024,2048]{1,0:T(8,128)(2,1)} %param.30, bf16[64,512]{1,0:T(8,128)(2,1)S(1)} %bitcast.176, bf16[64,512]{1,0:T(8,128)(2,1)S(1)} %bitcast.177, bf16[64,2048]{1,0:T(8,128)(2,1)S(1)} %copy-done.4), kind=kOutput, calls=%fused_computation.75 | convolution fusion | flops 269483968 | bytes 5112064 | tf_op jit(solution)/shard_map/dot_general | solution.py:147
  124.1 0.1 multiply_convert_fusion.1
  124.2 2.3 gather_fusion
  126.6 1.6 broadcast_in_dim.49
  128.2 46.2 %scatter_fusion = bf16[32,16,2048]{2,1,0:T(8,128)(2,1)} fusion(bf16[32,16,2048]{2,1,0:T(8,128)(2,1)} %broadcast_in_dim.49, s32[256]{0:T(256)S(1)} %bitcast.172, bf16[256,2048]{1,0:T(8,128)(2,1)} %gather_fusion), kind=kCustom, calls=%fused_computation.2 | custom fusion | bytes 3147776 | tf_op jit(solution)/shard_map/scatter | solution.py:172
  174.4 51.9 %all_to_all.40 = bf16[32,16,2048]{2,1,0:T(8,128)(2,1)S(1)} all-to-all(bf16[32,16,2048]{2,1,0:T(8,128)(2,1)} %scatter_fusion), channel_id=1, replica_groups=mesh['sp'=8,'tp'=4] {'sp','tp'}, dimensions={0} | all-to-all | bytes 4194304 | tf_op jit(solution)/shard_map/all_to_all | solution.py:174
  226.3 1.3 copy-done.3
  227.7 3.6 %fusion.4 = f32[512,1024]{1,0:T(8,128)} fusion(bf16[512,2048]{1,0:T(8,128)(2,1)S(1)} %bitcast.174, bf16[1,2048,1024]{2,1,0:T(8,128)(2,1)S(1)} %copy-done.8), kind=kOutput, calls=%fused_computation.7 | convolution fusion | flops 2147483648 | bytes 8388608 | tf_op jit(solution)/shard_map/dot_general | solution.py:14
  231.3 10.6 %fusion.6 = bf16[512,2048]{1,0:T(8,128)(2,1)} fusion(bf16[1,1024,2048]{2,1,0:T(8,128)(2,1)} %param.36, f32[512,1024]{1,0:T(8,128)} %fusion.4, bf16[512,2048]{1,0:T(8,128)(2,1)} %bitcast.175, bf16[1,2048,1024]{2,1,0:T(8,128)(2,1)} %param.35), kind=kOutput, calls=%fused_computation.9 | convolution fusion | flops 4299161600 | bytes 14680064 | tf_op jit(solution)/shard_map/dot_general | solution.py:17
  241.9 3.7 %all-to-all-start.3 = ((bf16[32,16,2048]{2,1,0:T(8,128)(2,1)}), bf16[32,16,2048]{2,1,0:T(8,128)(2,1)}, u32[]{:S(2)}, u32[]{:S(2)}) async-start(bf16[32,16,2048]{2,1,0:T(8,128)(2,1)} %bitcast.173), calls=%async_computation.3 | async-start | bytes 4194304 | tf_op jit(solution)/shard_map/all_to_all | solution.py:181
  245.6 0.7 copy.45
  246.3 2.1 fusion.98
  248.4 45.9 %all-to-all-done.3 = bf16[32,16,2048]{2,1,0:T(8,128)(2,1)} async-done(((bf16[32,16,2048]{2,1,0:T(8,128)(2,1)}), bf16[32,16,2048]{2,1,0:T(8,128)(2,1)}, u32[]{:S(2)}, u32[]{:S(2)}) %all-to-all-start.3) | async-done | bytes 2097184 | tf_op jit(solution)/shard_map/all_to_all | solution.py:181
  294.3 5.1 %gather_fusion.1 = bf16[256,2048]{1,0:T(8,128)(2,1)} fusion(bf16[32,16,2048]{2,1,0:T(8,128)(2,1)} %all-to-all-done.3, s32[256]{0:T(256)S(1)} %bitcast.171), kind=kCustom, calls=%fused_computation.1 | custom fusion | bytes 2099200 | tf_op jit(solution)/shard_map/gather | solution.py:182
  299.5 2.7 reshape.410
  302.2 3.2 %multiply_reduce_fusion = f32[64,2048]{1,0:T(8,128)S(1)} fusion(f32[64,4,2048]{2,1,0:T(4,128)} %reshape.410, f32[64,4]{1,0:T(8,128)} %copy.45), kind=kLoop, calls=%fused_computation.26 | loop fusion | flops 917504 | bytes 2622464 | tf_op jit(solution)/shard_map/reduce_sum | solution.py:183
  305.4 3.2 %fusion.16 = bf16[64,2048]{1,0:T(8,128)(2,1)} fusion(f32[64,2048]{1,0:T(8,128)S(1)} %multiply_reduce_fusion, f32[64,2048]{1,0:T(8,128)S(1)} %get-tuple-element.97, bf16[512,2048]{1,0:T(8,128)(2,1)S(1)} %copy-done, bf16[64,2048]{1,0:T(8,128)(2,1)S(1)} %multiply_convert_fusion.1, bf16[2048,512]{1,0:T(8,128)(2,1)} %param.38, f32[64,512]{1,0:T(8,128)S(1)} %fusion.98), kind=kOutput, calls=%fused_computation.23 | convolution fusion | flops 269025280 | bytes 5898240 | tf_op jit(solution)/shard_map/dot_general | solution.py:17
  (54 shorter events, 0.9 us)
Async XLA Ops:
  6.5 298.9 %copy-start = (bf16[512,2048]{1,0:T(8,128)(2,1)S(1)}, bf16[512,2048]{1,0:T(8,128)(2,1)}, u32[]{:S(2)}) copy-start(bf16[512,2048]{1,0:T(8,128)(2,1)} %param.39) | copy-start | bytes 6291460
  6.5 48.0 %all-gather.3.cloned.1.call-start = ((), (), s32[]{:S(2)}) async-start(), calls=%async_computation.4 | async-start | bytes 1179648 | tf_op jit(solution)/shard_map/all_gather | solution.py:102
  8.2 49.4 %copy-start.12 = (bf16[256,1,128]{2,0,1:T(8,128)(2,1)S(1)}, bf16[256,1,128]{2,0,1:T(8,128)(2,1)}, u32[]{:S(2)}) copy-start(bf16[256,1,128]{2,0,1:T(8,128)(2,1)} %param.21) | copy-start | bytes 196612
  8.3 87.5 %all-gather.5.cloned.1.call-start = ((), (), s32[]{:S(2)}) async-start(), calls=%async_computation.5 | async-start | bytes 1179648 | tf_op jit(solution)/shard_map/all_gather | solution.py:113
  54.6 3.1 copy-start.9
  57.6 38.2 %copy-start.11 = (bf16[256,1,256]{2,0,1:T(8,128)(2,1)S(1)}, bf16[256,1,256]{2,0,1:T(8,128)(2,1)}, u32[]{:S(2)}) copy-start(bf16[256,1,256]{2,0,1:T(8,128)(2,1)} %param.24) | copy-start | bytes 393220
  95.8 3.5 %copy-start.2 = (f32[256,2048]{0,1:T(8,128)S(1)}, f32[256,2048]{0,1:T(8,128)}, u32[]{:S(2)}) copy-start(f32[256,2048]{0,1:T(8,128)} %get-tuple-element.62) | copy-start | bytes 6291460
  97.5 1.8 copy-start.1
  101.4 1.2 copy-start.10
  103.1 0.7 copy-start.7
  103.7 17.2 %copy-start.4 = (bf16[64,2048]{1,0:T(8,128)(2,1)S(1)}, bf16[64,2048]{1,0:T(8,128)(2,1)}, u32[]{:S(2)}) copy-start(bf16[64,2048]{1,0:T(8,128)(2,1)} %param.20) | copy-start | bytes 786436
  106.0 7.4 %all-to-all-start.1 = ((bf16[4,2,4096]{2,1,0:T(2,128)(2,1)}), bf16[4,2,4096]{2,1,0:T(2,128)(2,1)S(1)}, u32[]{:S(2)}, u32[]{:S(2)}) async-start(bf16[4,2,4096]{2,1,0:T(2,128)(2,1)} %reshape.432), calls=%async_computation.1 | async-start | bytes 131072 | tf_op jit(solution)/shard_map/all_to_all | solution.py:144
  113.4 7.4 %all-to-all-start = ((bf16[4,2,4096]{2,1,0:T(2,128)(2,1)}), bf16[4,2,4096]{2,1,0:T(2,128)(2,1)S(1)}, u32[]{:S(2)}, u32[]{:S(2)}) async-start(bf16[4,2,4096]{2,1,0:T(2,128)(2,1)} %reshape.434), calls=%async_computation | async-start | bytes 131072 | tf_op jit(solution)/shard_map/all_to_all | solution.py:143
  120.9 3.2 %copy-start.5 = (f32[2048]{0:T(1024)S(1)}, f32[2048]{0:T(1024)}, u32[]{:S(2)}) copy-start(f32[2048]{0:T(1024)} %param.31) | copy-start | bytes 24580
  174.4 53.2 %copy-start.8 = (bf16[1,2048,1024]{2,1,0:T(8,128)(2,1)S(1)}, bf16[1,2048,1024]{2,1,0:T(8,128)(2,1)}, u32[]{:S(2)}) copy-start(bf16[1,2048,1024]{2,1,0:T(8,128)(2,1)} %param.34) | copy-start | bytes 12582916
  226.3 1.3 copy-start.3
  241.9 3.7 %copy-start.6 = (f32[64,4]{0,1:T(4,128)S(1)}, f32[64,4]{0,1:T(4,128)}, u32[]{:S(2)}) copy-start(f32[64,4]{0,1:T(4,128)} %param.33) | copy-start | bytes 3076
  241.9 52.4 %all-to-all-start.3 = ((bf16[32,16,2048]{2,1,0:T(8,128)(2,1)}), bf16[32,16,2048]{2,1,0:T(8,128)(2,1)}, u32[]{:S(2)}, u32[]{:S(2)}) async-start(bf16[32,16,2048]{2,1,0:T(8,128)(2,1)} %bitcast.173), calls=%async_computation.3 | async-start | bytes 4194304 | tf_op jit(solution)/shard_map/all_to_all | solution.py:181
Sparse Core Ops, SparseCore 0:
  9.5 44.9 all-gather.2
  56.7 39.0 all-gather.4
